TPU v7x, 32 devices: a whole 2x2x4 slice. The times are simulated.
32 devices in a mesh: grp: 2 (over y), sp: 4 (over z), tp: 4 (over x, core).
Axes of the slice: x: 2, y: 2, z: 4, core: 2. Of those that a mesh axis runs over, the one named last changes fastest.
Arguments:
- hidden_in: bfloat16 [5120, 4096], P(('grp', 'sp'), 'tp'), parts along dimension 0, may hold values from -64 to 64
- norm_gain: float32 [2, 4096], replicated, may hold values from 0.1 to 1.9
- w_pool_in: bfloat16 [2, 4096, 1024], P(None, 'sp', 'tp'), may hold values from -0.09375 to 0.09375
- w_pool_gate: bfloat16 [2, 4096, 1024], P(None, 'sp', 'tp'), may hold values from -0.09375 to 0.09375
- group_mix: bfloat16 [2, 16, 64, 64], replicated, may hold values from -0.75 to 0.75
- w_out: bfloat16 [2, 1024, 4096], P(None, 'sp', 'tp'), may hold values from -0.1875 to 0.1875
Outputs:
- hidden_out: bfloat16 [5120, 4096], P(('grp', 'sp'), 'tp'), parts along dimension 0
There are 2 independent parts, one for each index of `grp`. A program takes and returns all parts, laid end to end along the dimension named above; an argument that names none is the same for every part. Nothing has to cross between parts.
All inputs are finite; a program needn't handle non-finite values.
Results may differ from a plain program's by a relative error of at most 0.012.
Values may be sent and summed in bfloat16 or wider, within the bound.
A program may use at most 64 MiB of HBM per device.

v0:
```python
import jax
import jax.numpy as jnp
from jax import lax
from jax.sharding import PartitionSpec as P

GROUP = 64
norm_eps = 1e-06


def with_halo(array, sides, width):
    for axis, dim in sides:
        size, length = (lax.axis_size(axis), array.shape[dim])
        up = [(i, (i + 1) % size) for i in range(size - 1)]
        down = [(j, i) for i, j in up]
        last = lax.slice_in_dim(array, length - width, length, axis=dim)
        leading = lax.slice_in_dim(array, 0, width, axis=dim)
        before = lax.ppermute(last, axis, up)
        after = lax.ppermute(leading, axis, down)
        array = jnp.concatenate([before, array, after], axis=dim)
    return array


def local(hidden_in, norm_gain, w_pool_in, w_pool_gate, group_mix, w_out):
    tok_rows = hidden_in.shape[0]
    col_count = hidden_in.shape[1]
    chan_count = w_pool_in.shape[2]
    group_local = chan_count // GROUP
    layer_count = w_pool_in.shape[0]
    col_rank = lax.axis_index("tp")
    row_rank = lax.axis_index("sp")
    total_rows = tok_rows * lax.axis_size("sp")
    full_width = col_count * lax.axis_size("tp")
    position = row_rank * tok_rows + jnp.arange(tok_rows, dtype=jnp.int32)
    channel_code = (col_rank * group_local + jnp.arange(chan_count, dtype=jnp.int32) // GROUP) % 4
    every_in, every_gate, every_out = (
        lax.all_gather(w_pool_in, "sp", axis=1, tiled=True),
        lax.all_gather(w_pool_gate, "sp", axis=1, tiled=True),
        lax.all_gather(w_out, "sp", axis=1, tiled=True),
    )
    resid = hidden_in
    for layer in range(layer_count):
        weight_in = every_in[layer]
        weight_gate = every_gate[layer]
        weight_out = every_out[layer]
        resid_f = resid.astype(jnp.float32)
        squares = lax.psum(jnp.sum(resid_f * resid_f, axis=1), "tp")
        scaling = lax.rsqrt(squares / full_width + norm_eps)
        own_gain = lax.dynamic_slice_in_dim(norm_gain[layer], col_rank * col_count, col_count)
        normed = (resid_f * scaling[:, None] * own_gain[None, :]).astype(jnp.bfloat16)
        piece = lax.all_gather(normed, "tp", axis=1, tiled=True)
        pool_sum = jnp.dot(piece, weight_in, preferred_element_type=jnp.float32)
        gate_sum = jnp.dot(piece, weight_gate, preferred_element_type=jnp.float32)
        pool_in = pool_sum.astype(jnp.bfloat16)
        gate = gate_sum.astype(jnp.bfloat16)
        padded = with_halo(pool_in, (("sp", 0),), 8).astype(jnp.float32)
        running = jnp.zeros((tok_rows, chan_count), jnp.float32)
        averaged = jnp.zeros((tok_rows, chan_count), jnp.float32)
        previous = 0
        for code_value, half in enumerate((1, 2, 4, 8)):
            for offset in list(range(-half, -previous)) + list(range(previous, half)):
                running = running + padded[8 + offset : 8 + offset + tok_rows]
            previous = half
            counted = (
                jnp.minimum(position + half, total_rows) - jnp.maximum(position - half, 0)
            ).astype(jnp.float32)
            averaged = jnp.where(
                channel_code[None, :] == code_value, running / counted[:, None], averaged
            )
        pooled = (averaged - padded[8 : 8 + tok_rows]).astype(jnp.bfloat16)
        own_mix = lax.dynamic_slice_in_dim(group_mix[layer], col_rank * group_local, group_local, 0)
        mixed = jnp.einsum(
            "tgc,gcd->tgd",
            pooled.reshape(tok_rows, group_local, GROUP),
            own_mix,
            preferred_element_type=jnp.float32,
        ).reshape(tok_rows, chan_count)
        branch = (mixed * jax.nn.silu(gate.astype(jnp.float32))).astype(jnp.bfloat16)
        projected = jnp.dot(
            lax.all_gather(branch, "tp", axis=1, tiled=True),
            weight_out,
            preferred_element_type=jnp.float32,
        )
        resid = (resid_f + projected).astype(jnp.bfloat16)
    return resid


def solution(mesh):
    in_specs = (
        P(("grp", "sp"), "tp"),
        P(),
        P(None, "sp", "tp"),
        P(None, "sp", "tp"),
        P(),
        P(None, "sp", "tp"),
    )
    out_specs = P(("grp", "sp"), "tp")
    return jax.shard_map(local, mesh=mesh, in_specs=in_specs, out_specs=out_specs, check_vma=False)
```

profile of v0, /device:TPU:0, one launch (start us, length us, event | category | flops | bytes accessed | tf_op | source)
XLA Modules:
  0.0 417.1 jit_solution(7042506414387707074)
XLA Ops:
  6.5 0.0 copy-start
  6.5 0.0 all-gather.10.cloned.1.call-start
  6.5 0.7 all-gather.10.cloned.1.call-update
  7.3 0.0 all-gather.8.cloned.1.call-start
  7.3 1.6 fusion
  9.0 8.4 %psum.14 = f32[640]{0:T(1024)S(1)} all-reduce(f32[640]{0:T(1024)S(1)} %fusion), channel_id=1, replica_groups=mesh['grp'=2,'sp'=4,'tp'=4] {'tp'}, use_global_device_ids=true, to_apply=%region_1.2 | all-reduce | flops 640 | bytes 5120 | tf_op jit(solution)/shard_map/psum | solution.py:46
  17.3 0.9 fusion.41
  18.2 0.0 copy-done
  18.2 0.0 copy-start.1
  18.2 1.4 fusion.2
  19.7 0.0 all-gather.8.cloned.1.call-update
  19.7 0.0 all-gather.12.cloned.1.call-start
  19.7 0.7 all-gather.12.cloned.1.call-update
  20.4 0.0 all-gather.16.cloned.1.call-start
  20.5 0.5 all-gather.16.cloned.1.call-update
  21.0 0.0 all-gather.14.cloned.1.call-start
  21.1 0.0 copy-done.1
  21.2 71.2 %all-gather.10.cloned.1.call-done = bf16[2,4096,256]{2,1,0:T(8,128)(2,1)} async-done(((bf16[2,1024,256]{2,1,0:T(8,128)(2,1)}), bf16[2,4096,256]{2,1,0:T(8,128)(2,1)}) %all-gather.10.cloned.1.call-update) | async-done | bytes 4194320 | tf_op jit(solution)/shard_map/all_gather | solution.py:36
  92.4 40.5 %all-gather.8.cloned.1.call-done = bf16[640,4096]{1,0:T(8,128)(2,1)} async-done(((bf16[640,1024]{1,0:T(8,128)(2,1)}), bf16[640,4096]{1,0:T(8,128)(2,1)}) %all-gather.8.cloned.1.call-update) | async-done | bytes 5242896 | tf_op jit(solution)/shard_map/all_gather | solution.py:50
  132.9 4.7 %fusion.14 = bf16[640,256]{1,0:T(8,128)(2,1)S(1)} fusion(bf16[640,4096]{1,0:T(8,128)(2,1)} %all-gather.8.cloned.1.call-done, bf16[2,4096,256]{2,1,0:T(8,128)(2,1)} %all-gather.10.cloned.1.call-done), kind=kOutput, calls=%fused_computation.26 | convolution fusion | flops 1342341120 | bytes 7667712 | tf_op jit(solution)/shard_map/dot_general | solution.py:51
  137.6 3.4 collective-permute-start
  141.0 1.3 collective-permute-start.1
  142.3 0.0 collective-permute-done
  142.3 4.2 %collective-permute-done.1 = bf16[8,256]{1,0:T(8,128)(2,1)S(1)} collective-permute-done((bf16[8,256]{1,0:T(8,128)(2,1)S(1)}, bf16[8,256]{1,0:T(8,128)(2,1)S(1)}, u32[]{:S(2)}, u32[]{:S(2)}) %collective-permute-start.1) | collective-permute-done | bytes 4128 | tf_op jit(solution)/shard_map/ppermute | solution.py:18
  146.5 1.5 fusion.26
  148.0 0.2 copy.14
  148.2 0.3 fusion.30
  148.5 0.2 copy.15
  148.7 66.5 %all-gather.12.cloned.1.call-done = bf16[2,4096,256]{2,1,0:T(8,128)(2,1)} async-done(((bf16[2,1024,256]{2,1,0:T(8,128)(2,1)}), bf16[2,4096,256]{2,1,0:T(8,128)(2,1)}) %all-gather.12.cloned.1.call-update) | async-done | bytes 4194320 | tf_op jit(solution)/shard_map/all_gather | solution.py:37
  215.3 5.4 %multiply_convert_fusion.1 = bf16[640,256]{1,0:T(8,128)(2,1)} fusion(f32[640,256]{1,0:T(8,128)S(1)} %copy.15, bf16[640,4096]{1,0:T(8,128)(2,1)} %all-gather.8.cloned.1.call-done, bf16[2,4096,256]{2,1,0:T(8,128)(2,1)} %all-gather.12.cloned.1.call-done), kind=kOutput, calls=%fused_computation.69 | convolution fusion | flops 1343488000 | bytes 8323072 | tf_op jit(solution)/shard_map/dot_general | solution.py:52
  220.7 0.0 all-gather.14.cloned.1.call-update
  220.7 0.0 all-gather.18.cloned.1.call-start
  220.8 75.1 %all-gather.16.cloned.1.call-done = bf16[2,1024,1024]{2,1,0:T(8,128)(2,1)} async-done(((bf16[2,256,1024]{2,1,0:T(8,128)(2,1)}), bf16[2,1024,1024]{2,1,0:T(8,128)(2,1)}) %all-gather.16.cloned.1.call-update) | async-done | bytes 4194320 | tf_op jit(solution)/shard_map/all_gather | solution.py:38
  295.9 18.2 %all-gather.14.cloned.1.call-done = bf16[640,1024]{1,0:T(8,128)(2,1)} async-done(((bf16[640,256]{1,0:T(8,128)(2,1)}), bf16[640,1024]{1,0:T(8,128)(2,1)}) %all-gather.14.cloned.1.call-update) | async-done | bytes 1310736 | tf_op jit(solution)/shard_map/all_gather | solution.py:79
  314.1 3.7 fusion.4
  317.8 5.9 %psum.15 = f32[640]{0:T(1024)S(1)} all-reduce(f32[640]{0:T(1024)S(1)} %get-tuple-element.13), channel_id=1, replica_groups=mesh['grp'=2,'sp'=4,'tp'=4] {'tp'}, use_global_device_ids=true, to_apply=%region_3.4 | all-reduce | flops 640 | bytes 5120 | tf_op jit(solution)/shard_map/psum | solution.py:46
  323.7 1.4 fusion.6
  325.2 0.0 all-gather.18.cloned.1.call-update
  325.2 0.0 all-gather.20.cloned.1.call-start
  325.2 41.6 %all-gather.18.cloned.1.call-done = bf16[640,4096]{1,0:T(8,128)(2,1)} async-done(((bf16[640,1024]{1,0:T(8,128)(2,1)}), bf16[640,4096]{1,0:T(8,128)(2,1)}) %all-gather.18.cloned.1.call-update) | async-done | bytes 5242896 | tf_op jit(solution)/shard_map/all_gather | solution.py:50
  366.8 4.7 %fusion.17 = bf16[640,256]{1,0:T(8,128)(2,1)S(1)} fusion(bf16[640,4096]{1,0:T(8,128)(2,1)} %all-gather.18.cloned.1.call-done, bf16[2,4096,256]{2,1,0:T(8,128)(2,1)} %all-gather.10.cloned.1.call-done), kind=kOutput, calls=%fused_computation.29 | convolution fusion | flops 1342341120 | bytes 7667712 | tf_op jit(solution)/shard_map/dot_general | solution.py:51
  371.5 3.4 collective-permute-start.2
  374.9 1.5 collective-permute-start.3
  376.4 0.0 collective-permute-done.2
  376.4 4.0 collective-permute-done.3
  380.5 1.5 fusion.27
  381.9 0.2 copy.17
  382.1 0.3 fusion.28
  382.4 0.2 copy.18
  382.7 5.4 %multiply_convert_fusion = bf16[640,256]{1,0:T(8,128)(2,1)} fusion(f32[640,256]{1,0:T(8,128)S(1)} %copy.18, bf16[640,4096]{1,0:T(8,128)(2,1)} %all-gather.18.cloned.1.call-done, bf16[2,4096,256]{2,1,0:T(8,128)(2,1)} %all-gather.12.cloned.1.call-done), kind=kOutput, calls=%fused_computation.68 | convolution fusion | flops 1343488000 | bytes 8323072 | tf_op jit(solution)/shard_map/dot_general | solution.py:52
  388.1 0.0 all-gather.20.cloned.1.call-update
  388.1 17.6 %all-gather.20.cloned.1.call-done = bf16[640,1024]{1,0:T(8,128)(2,1)} async-done(((bf16[640,256]{1,0:T(8,128)(2,1)}), bf16[640,1024]{1,0:T(8,128)(2,1)}) %all-gather.20.cloned.1.call-update) | async-done | bytes 1310736 | tf_op jit(solution)/shard_map/all_gather | solution.py:79
  405.7 4.6 %fusion.7 = bf16[640,1024]{1,0:T(8,128)(2,1)} fusion(bf16[640,1024]{1,0:T(8,128)(2,1)S(1)} %get-tuple-element.14, bf16[640,1024]{1,0:T(8,128)(2,1)} %all-gather.20.cloned.1.call-done, bf16[2,1024,1024]{2,1,0:T(8,128)(2,1)} %all-gather.16.cloned.1.call-done), kind=kOutput, calls=%fused_computation.13 | convolution fusion | flops 1344143360 | bytes 6029312 | tf_op jit(solution)/shard_map/dot_general | solution.py:78
  (13 shorter events, 0.2 us)
Async XLA Ops:
  6.5 11.7 %copy-start = (bf16[640,1024]{1,0:T(8,128)(2,1)S(1)}, bf16[640,1024]{1,0:T(8,128)(2,1)}, u32[]{:S(2)}) copy-start(bf16[640,1024]{1,0:T(8,128)(2,1)} %param.6) | copy-start | bytes 3932164
  6.5 85.9 %all-gather.10.cloned.1.call-start = ((), (), s32[]{:S(2)}) async-start(), calls=%async_computation.1 | async-start | bytes 5242880 | tf_op jit(solution)/shard_map/all_gather | solution.py:36
  7.3 125.6 %all-gather.8.cloned.1.call-start = ((), (), s32[]{:S(2)}) async-start(), calls=%async_computation | async-start | bytes 6553600 | tf_op jit(solution)/shard_map/all_gather | solution.py:50
  18.2 2.9 copy-start.1
  19.7 195.6 %all-gather.12.cloned.1.call-start = ((), (), s32[]{:S(2)}) async-start(), calls=%async_computation.2 | async-start | bytes 5242880 | tf_op jit(solution)/shard_map/all_gather | solution.py:37
  20.4 275.5 %all-gather.16.cloned.1.call-start = ((), (), s32[]{:S(2)}) async-start(), calls=%async_computation.4 | async-start | bytes 5242880 | tf_op jit(solution)/shard_map/all_gather | solution.py:38
  21.0 293.1 %all-gather.14.cloned.1.call-start = ((), (), s32[]{:S(2)}) async-start(), calls=%async_computation.3 | async-start | bytes 1638400 | tf_op jit(solution)/shard_map/all_gather | solution.py:79
  137.6 4.7 %collective-permute-start = (bf16[8,256]{1,0:T(8,128)(2,1)S(1)}, bf16[8,256]{1,0:T(8,128)(2,1)S(1)}, u32[]{:S(2)}, u32[]{:S(2)}) collective-permute-start(bf16[8,256]{1,0:T(8,128)(2,1)S(1)} %get-tuple-element.9), channel_id=1, source_target_pairs={{0,4},{4,8},{8,12},{1,5},{5,9},{9,13},{2,6},{6,10},{10,14},{3,7},{... | collective-permute-start | bytes 12296 | tf_op jit(solution)/shard_map/ppermute | solution.py:17
  141.0 5.5 %collective-permute-start.1 = (bf16[8,256]{1,0:T(8,128)(2,1)S(1)}, bf16[8,256]{1,0:T(8,128)(2,1)S(1)}, u32[]{:S(2)}, u32[]{:S(2)}) collective-permute-start(bf16[8,256]{1,0:T(8,128)(2,1)S(1)} %get-tuple-element.10), channel_id=1, source_target_pairs={{4,0},{8,4},{12,8},{5,1},{9,5},{13,9},{6,2},{10,6},{14,10},{7,3},{... | collective-permute-start | bytes 12296 | tf_op jit(solution)/shard_map/ppermute | solution.py:18
  220.7 146.1 %all-gather.18.cloned.1.call-start = ((), (), s32[]{:S(2)}) async-start(), calls=%async_computation.5 | async-start | bytes 6553600 | tf_op jit(solution)/shard_map/all_gather | solution.py:50
  325.2 80.5 %all-gather.20.cloned.1.call-start = ((), (), s32[]{:S(2)}) async-start(), calls=%async_computation.6 | async-start | bytes 1638400 | tf_op jit(solution)/shard_map/all_gather | solution.py:79
  371.5 4.9 %collective-permute-start.2 = (bf16[8,256]{1,0:T(8,128)(2,1)S(1)}, bf16[8,256]{1,0:T(8,128)(2,1)S(1)}, u32[]{:S(2)}, u32[]{:S(2)}) collective-permute-start(bf16[8,256]{1,0:T(8,128)(2,1)S(1)} %get-tuple-element.7), channel_id=1, source_target_pairs={{0,4},{4,8},{8,12},{1,5},{5,9},{9,13},{2,6},{6,10},{10,14},{3,7},{... | collective-permute-start | bytes 12296 | tf_op jit(solution)/shard_map/ppermute | solution.py:17
  374.9 5.5 %collective-permute-start.3 = (bf16[8,256]{1,0:T(8,128)(2,1)S(1)}, bf16[8,256]{1,0:T(8,128)(2,1)S(1)}, u32[]{:S(2)}, u32[]{:S(2)}) collective-permute-start(bf16[8,256]{1,0:T(8,128)(2,1)S(1)} %get-tuple-element.8), channel_id=1, source_target_pairs={{4,0},{8,4},{12,8},{5,1},{9,5},{13,9},{6,2},{10,6},{14,10},{7,3},{... | collective-permute-start | bytes 12296 | tf_op jit(solution)/shard_map/ppermute | solution.py:18
Sparse Core Ops, SparseCore 0:
  8.9 83.4 all-gather.9
  94.0 38.8 all-gather.7
  134.5 80.7 all-gather.11
  216.7 79.1 all-gather.15
  297.3 16.7 all-gather.13
  325.3 41.4 all-gather.17
  388.2 17.3 all-gather.19
where the time goes:
time: 417 us
  waiting for transfers between devices  341 us (82%)
  matrix products  29 us (7%)
  blocking collectives  14.3 us (3%)
  between operations  13.7 us (3%)
  starting transfers between devices  9.78 us (2%)
  other arithmetic  7.59 us (2%)
    all_gather x2, waiting for transfers between devices, local(): piece = lax.all_gather(normed, 'tp', axis=1, tiled=True)  82.1 us
    all_gather x1, waiting for transfers between devices, local(): lax.all_gather(w_out, 'sp', axis=1, tiled=True)  75.1 us
    all_gather x1, waiting for transfers between devices, local(): lax.all_gather(w_pool_in, 'sp', axis=1, tiled=True)  71.2 us
    all_gather x1, waiting for transfers between devices, local(): lax.all_gather(w_pool_gate, 'sp', axis=1, tiled=True)  66.5 us
    all_gather x2, waiting for transfers between devices, local(): lax.all_gather(branch, 'tp', axis=1, tiled=True)  35.8 us
    psum x2, blocking collectives, local(): squares = lax.psum(jnp.sum(resid_f * resid_f, axis=1), 'tp')  14.3 us
    dot_general x2, matrix products, local(): gate_sum = jnp.dot(piece, weight_gate, preferred_element_type=jnp.float32)  10.9 us
    dot_general x2, matrix products, local(): pool_sum = jnp.dot(piece, weight_in, preferred_element_type=jnp.float32)  9.35 us
  transfers between devices with their start and end apart: 11, of which 9 were waited for; matrix products, arithmetic and copies ran while one was open for 4% of the time, Pallas kernels for 0%

commit v1 on v0

--- a/solution.py
+++ b/solution.py
@@ -47,7 +47,14 @@
         scaling = lax.rsqrt(squares / full_width + norm_eps)
         own_gain = lax.dynamic_slice_in_dim(norm_gain[layer], col_rank * col_count, col_count)
         normed = (resid_f * scaling[:, None] * own_gain[None, :]).astype(jnp.bfloat16)
-        piece = lax.all_gather(normed, "tp", axis=1, tiled=True)
+        ring = [normed]
+        for hop in range(3):
+            ring.append(lax.ppermute(ring[-1], "tp", [(dev, (dev + 1) % 4) for dev in range(4)]))
+        piece = jnp.roll(
+            jnp.concatenate(ring[::-1], axis=1),
+            (lax.axis_index("tp") + 1) * ring[0].shape[1],
+            axis=1,
+        )
         pool_sum = jnp.dot(piece, weight_in, preferred_element_type=jnp.float32)
         gate_sum = jnp.dot(piece, weight_gate, preferred_element_type=jnp.float32)
         pool_in = pool_sum.astype(jnp.bfloat16)

time: 417 us -> 392 us (0.940)
  waiting for transfers between devices: 341 us -> 301 us
  other arithmetic: 7.59 us -> 25.1 us
    ppermute x0 -> x6, waiting for transfers between devices: none -> 102 us  [local(): lax.ppermute(ring[-1], 'tp', [(dev, (dev + 1) % 4) for dev in range(4)])]
    all_gather x2 -> x0, waiting for transfers between devices: 82.1 us -> none  [local(): piece = lax.all_gather(normed, 'tp', axis=1, tiled=True)]
    all_gather x1, waiting for transfers between devices: 71.2 us -> 10.4 us  [local(): lax.all_gather(w_pool_in, 'sp', axis=1, tiled=True)]
    concatenate x0 -> x2, other arithmetic: none -> 19.7 us  [local(): jnp.roll(jnp.concatenate(ring[::-1], axis=1), (lax.axis_index('tp') + 1)...]
  transfers between devices with their start and end apart: 11 -> 15, of which waited for: 9 -> 13; matrix products, arithmetic and copies ran while one was open for 4% -> 7% of each run, Pallas kernels for 0% -> 0%
where the time goes in v1:
time: 392 us; the launch traced here: 391 us
  waiting for transfers between devices  301 us (77%)
  matrix products  26.7 us (7%)
  other arithmetic  25.1 us (6%)
  blocking collectives  14.3 us (4%)
  between operations  13.4 us (3%)
  starting transfers between devices  7.7 us (2%)
    ppermute x6, waiting for transfers between devices, local(): lax.ppermute(ring[-1], 'tp', [(dev, (dev + 1) % 4) for dev in range(4)])  102 us
    all_gather x1, waiting for transfers between devices, local(): lax.all_gather(w_out, 'sp', axis=1, tiled=True)  75.3 us
    all_gather x1, waiting for transfers between devices, local(): lax.all_gather(w_pool_gate, 'sp', axis=1, tiled=True)  66.2 us
    all_gather x2, waiting for transfers between devices, local(): lax.all_gather(branch, 'tp', axis=1, tiled=True)  36.7 us
    concatenate x2, other arithmetic, local(): jnp.roll(jnp.concatenate(ring[::-1], axis=1), (lax.axis_index('tp') + 1)...  19.7 us
    psum x2, blocking collectives, local(): squares = lax.psum(jnp.sum(resid_f * resid_f, axis=1), 'tp')  14.3 us
    dot_general x2, matrix products, local(): gate_sum = jnp.dot(piece, weight_gate, preferred_element_type=jnp.float32)  10.9 us
    all_gather x1, waiting for transfers between devices, local(): lax.all_gather(w_pool_in, 'sp', axis=1, tiled=True)  10.4 us
  transfers between devices with their start and end apart: 15, of which 13 were waited for; matrix products, arithmetic and copies ran while one was open for 7% of the time, Pallas kernels for 0%

profile of v1, /device:TPU:0, one launch (start us, length us, event | category | flops | bytes accessed | tf_op | source)
XLA Modules:
  0.0 391.1 jit_solution(17403973731508083218)
XLA Ops:
  6.5 0.0 all-gather.6.cloned.1.call-start
  6.5 0.7 all-gather.6.cloned.1.call-update
  7.3 0.0 all-gather.8.cloned.1.call-start
  7.3 0.7 all-gather.8.cloned.1.call-update
  8.0 0.0 all-gather.12.cloned.1.call-start
  8.1 1.6 fusion.14
  9.7 8.4 %psum.14 = f32[640]{0:T(1024)S(1)} all-reduce(f32[640]{0:T(1024)S(1)} %fusion.14), channel_id=1, replica_groups=mesh['grp'=2,'sp'=4,'tp'=4] {'tp'}, use_global_device_ids=true, to_apply=%region_1.2 | all-reduce | flops 640 | bytes 5120 | tf_op jit(solution)/shard_map/psum | solution.py:46
  18.1 0.9 fusion.55
  19.0 0.0 copy-done
  19.0 0.4 fusion.16
  19.4 0.1 collective-permute-start
  19.4 17.1 %collective-permute-done = bf16[640,1024]{1,0:T(8,128)(2,1)} collective-permute-done((bf16[640,1024]{1,0:T(8,128)(2,1)S(1)}, bf16[640,1024]{1,0:T(8,128)(2,1)}, u32[]{:S(2)}, u32[]{:S(2)}) %collective-permute-start) | collective-permute-done | bytes 1310752 | tf_op jit(solution)/shard_map/ppermute | solution.py:52
  36.5 0.0 collective-permute-start.1
  36.5 0.0 all-gather.12.cloned.1.call-update
  36.6 0.0 all-gather.10.cloned.1.call-start
  36.6 17.3 %collective-permute-done.1 = bf16[640,1024]{1,0:T(8,128)(2,1)} collective-permute-done((bf16[640,1024]{1,0:T(8,128)(2,1)}, bf16[640,1024]{1,0:T(8,128)(2,1)}, u32[]{:S(2)}, u32[]{:S(2)}) %collective-permute-start.1) | collective-permute-done | bytes 1310752 | tf_op jit(solution)/shard_map/ppermute | solution.py:52
  53.9 0.0 collective-permute-start.2
  53.9 0.0 copy-done.2
  54.0 0.7 fusion.52
  54.7 16.5 %collective-permute-done.2 = bf16[640,1024]{1,0:T(8,128)(2,1)} collective-permute-done((bf16[640,1024]{1,0:T(8,128)(2,1)}, bf16[640,1024]{1,0:T(8,128)(2,1)}, u32[]{:S(2)}, u32[]{:S(2)}) %collective-permute-start.2) | collective-permute-done | bytes 1310752 | tf_op jit(solution)/shard_map/ppermute | solution.py:52
  71.2 10.7 %fusion.10 = bf16[640,4096]{1,0:T(8,128)(2,1)} fusion(s32[]{:T(128)S(6)} %select_n.95, bf16[640,1024]{1,0:T(8,128)(2,1)} %collective-permute-done.2, bf16[640,1024]{1,0:T(8,128)(2,1)} %collective-permute-done.1, bf16[640,1024]{1,0:T(8,128)(2,1)} %collective-permute-done, bf16[640,1024]{1,0:T(8,128)(2,1)S(1)} %fusion.16), kind=kLoop, calls=%fused_computation.26 | loop fusion | flops 41943040 | bytes 10485764 | tf_op jit(solution)/shard_map/jit(_roll_dynamic)/concatenate | solution.py:53
  82.0 10.4 %all-gather.6.cloned.1.call-done = bf16[2,4096,256]{2,1,0:T(8,128)(2,1)} async-done(((bf16[2,1024,256]{2,1,0:T(8,128)(2,1)}), bf16[2,4096,256]{2,1,0:T(8,128)(2,1)}) %all-gather.6.cloned.1.call-update) | async-done | bytes 4194320 | tf_op jit(solution)/shard_map/all_gather | solution.py:36
  92.4 4.7 %fusion.28 = bf16[640,256]{1,0:T(8,128)(2,1)S(1)} fusion(bf16[640,4096]{1,0:T(8,128)(2,1)} %fusion.10, bf16[2,4096,256]{2,1,0:T(8,128)(2,1)} %all-gather.6.cloned.1.call-done), kind=kOutput, calls=%fused_computation.56 | convolution fusion | flops 1342341120 | bytes 7667712 | tf_op jit(solution)/shard_map/dot_general | solution.py:58
  97.1 1.3 collective-permute-start.3
  98.4 1.3 collective-permute-start.4
  99.7 0.0 collective-permute-done.3
  99.7 4.3 %collective-permute-done.4 = bf16[8,256]{1,0:T(8,128)(2,1)S(1)} collective-permute-done((bf16[8,256]{1,0:T(8,128)(2,1)S(1)}, bf16[8,256]{1,0:T(8,128)(2,1)S(1)}, u32[]{:S(2)}, u32[]{:S(2)}) %collective-permute-start.4) | collective-permute-done | bytes 4128 | tf_op jit(solution)/shard_map/ppermute | solution.py:18
  104.0 1.5 fusion.40
  105.5 0.2 copy.14
  105.7 1.1 fusion.44
  106.8 0.2 copy.15
  107.1 66.2 %all-gather.8.cloned.1.call-done = bf16[2,4096,256]{2,1,0:T(8,128)(2,1)} async-done(((bf16[2,1024,256]{2,1,0:T(8,128)(2,1)}), bf16[2,4096,256]{2,1,0:T(8,128)(2,1)}) %all-gather.8.cloned.1.call-update) | async-done | bytes 4194320 | tf_op jit(solution)/shard_map/all_gather | solution.py:37
  173.3 5.4 %multiply_convert_fusion.1 = bf16[640,256]{1,0:T(8,128)(2,1)} fusion(f32[640,256]{1,0:T(8,128)S(1)} %copy.15, bf16[640,4096]{1,0:T(8,128)(2,1)} %fusion.10, bf16[2,4096,256]{2,1,0:T(8,128)(2,1)} %all-gather.8.cloned.1.call-done), kind=kOutput, calls=%fused_computation.99 | convolution fusion | flops 1343488000 | bytes 8323072 | tf_op jit(solution)/shard_map/dot_general | solution.py:59
  178.7 0.0 all-gather.10.cloned.1.call-update
  178.7 0.0 all-gather.14.cloned.1.call-start
  178.8 75.3 %all-gather.12.cloned.1.call-done = bf16[2,1024,1024]{2,1,0:T(8,128)(2,1)} async-done(((bf16[2,256,1024]{2,1,0:T(8,128)(2,1)}), bf16[2,1024,1024]{2,1,0:T(8,128)(2,1)}) %all-gather.12.cloned.1.call-update) | async-done | bytes 4194320 | tf_op jit(solution)/shard_map/all_gather | solution.py:38
  254.1 18.2 %all-gather.10.cloned.1.call-done = bf16[640,1024]{1,0:T(8,128)(2,1)} async-done(((bf16[640,256]{1,0:T(8,128)(2,1)}), bf16[640,1024]{1,0:T(8,128)(2,1)}) %all-gather.10.cloned.1.call-update) | async-done | bytes 1310736 | tf_op jit(solution)/shard_map/all_gather | solution.py:86
  272.3 3.7 fusion.18
  276.0 5.9 %psum.15 = f32[640]{0:T(1024)S(1)} all-reduce(f32[640]{0:T(1024)S(1)} %get-tuple-element.14), channel_id=1, replica_groups=mesh['grp'=2,'sp'=4,'tp'=4] {'tp'}, use_global_device_ids=true, to_apply=%region_3.5 | all-reduce | flops 640 | bytes 5120 | tf_op jit(solution)/shard_map/psum | solution.py:46
  281.9 0.4 fusion.20
  282.3 0.0 copy-start.3
  282.3 0.1 collective-permute-start.5
  282.3 17.0 %collective-permute-done.5 = bf16[640,1024]{1,0:T(8,128)(2,1)S(1)} collective-permute-done((bf16[640,1024]{1,0:T(8,128)(2,1)S(1)}, bf16[640,1024]{1,0:T(8,128)(2,1)S(1)}, u32[]{:S(2)}, u32[]{:S(2)}) %collective-permute-start.5) | collective-permute-done | bytes 1310752 | tf_op jit(solution)/shard_map/ppermute | solution.py:52
  299.4 0.0 collective-permute-start.6
  299.4 17.0 %collective-permute-done.6 = bf16[640,1024]{1,0:T(8,128)(2,1)S(1)} collective-permute-done((bf16[640,1024]{1,0:T(8,128)(2,1)S(1)}, bf16[640,1024]{1,0:T(8,128)(2,1)S(1)}, u32[]{:S(2)}, u32[]{:S(2)}) %collective-permute-start.6) | collective-permute-done | bytes 1310752 | tf_op jit(solution)/shard_map/ppermute | solution.py:52
  316.4 0.0 collective-permute-start.7
  316.4 17.0 %collective-permute-done.7 = bf16[640,1024]{1,0:T(8,128)(2,1)S(1)} collective-permute-done((bf16[640,1024]{1,0:T(8,128)(2,1)S(1)}, bf16[640,1024]{1,0:T(8,128)(2,1)S(1)}, u32[]{:S(2)}, u32[]{:S(2)}) %collective-permute-start.7) | collective-permute-done | bytes 1310752 | tf_op jit(solution)/shard_map/ppermute | solution.py:52
  333.4 9.0 %fusion.3 = bf16[640,4096]{1,0:T(8,128)(2,1)S(1)} fusion(s32[]{:T(128)S(6)} %select_n.95, bf16[640,1024]{1,0:T(8,128)(2,1)S(1)} %collective-permute-done.7, bf16[640,1024]{1,0:T(8,128)(2,1)S(1)} %collective-permute-done.6, bf16[640,1024]{1,0:T(8,128)(2,1)S(1)} %collective-permute-done.5, bf16[640,1024]{1,0:T(8,128)(2,1)S(1)} %fusion.20), kind=kLoop, calls=%fused_computation.19 | loop fusion | flops 41943040 | bytes 10485764 | tf_op jit(solution)/shard_map/jit(_roll_dynamic)/concatenate | solution.py:53
  342.4 0.0 copy-done.3
  342.4 0.0 copy-start.1
  342.4 1.5 fusion.31
  343.9 0.8 copy-done.1
  344.8 3.5 collective-permute-start.8
  348.3 1.3 collective-permute-start.9
  349.6 0.0 collective-permute-done.8
  349.6 4.2 %collective-permute-done.9 = bf16[8,256]{1,0:T(8,128)(2,1)S(1)} collective-permute-done((bf16[8,256]{1,0:T(8,128)(2,1)S(1)}, bf16[8,256]{1,0:T(8,128)(2,1)S(1)}, u32[]{:S(2)}, u32[]{:S(2)}) %collective-permute-start.9) | collective-permute-done | bytes 4128 | tf_op jit(solution)/shard_map/ppermute | solution.py:18
  353.9 1.5 fusion.41
  355.3 0.2 copy.17
  355.6 0.3 fusion.42
  355.9 0.2 copy.18
  356.1 5.4 %multiply_convert_fusion = bf16[640,256]{1,0:T(8,128)(2,1)} fusion(f32[640,256]{1,0:T(8,128)S(1)} %copy.18, bf16[640,4096]{1,0:T(8,128)(2,1)} %copy-done.1, bf16[2,4096,256]{2,1,0:T(8,128)(2,1)} %all-gather.8.cloned.1.call-done), kind=kOutput, calls=%fused_computation.98 | convolution fusion | flops 1343488000 | bytes 8323072 | tf_op jit(solution)/shard_map/dot_general | solution.py:59
  361.5 0.0 all-gather.14.cloned.1.call-update
  361.5 18.5 %all-gather.14.cloned.1.call-done = bf16[640,1024]{1,0:T(8,128)(2,1)} async-done(((bf16[640,256]{1,0:T(8,128)(2,1)}), bf16[640,1024]{1,0:T(8,128)(2,1)}) %all-gather.14.cloned.1.call-update) | async-done | bytes 1310736 | tf_op jit(solution)/shard_map/all_gather | solution.py:86
  380.0 4.6 %fusion.21 = bf16[640,1024]{1,0:T(8,128)(2,1)} fusion(bf16[640,1024]{1,0:T(8,128)(2,1)S(1)} %get-tuple-element.15, bf16[640,1024]{1,0:T(8,128)(2,1)} %all-gather.14.cloned.1.call-done, bf16[2,1024,1024]{2,1,0:T(8,128)(2,1)} %all-gather.12.cloned.1.call-done), kind=kOutput, calls=%fused_computation.43 | convolution fusion | flops 1344143360 | bytes 6029312 | tf_op jit(solution)/shard_map/dot_general | solution.py:85
  (14 shorter events, 0.2 us)
Async XLA Ops:
  6.5 12.4 %copy-start = (bf16[640,1024]{1,0:T(8,128)(2,1)S(1)}, bf16[640,1024]{1,0:T(8,128)(2,1)}, u32[]{:S(2)}) copy-start(bf16[640,1024]{1,0:T(8,128)(2,1)} %param.8) | copy-start | bytes 3932164
  6.5 47.4 %copy-start.2 = (bf16[2,16,64,64]{3,2,1,0:T(8,128)(2,1)S(1)}, bf16[2,16,64,64]{3,2,1,0:T(8,128)(2,1)}, u32[]{:S(2)}) copy-start(bf16[2,16,64,64]{3,2,1,0:T(8,128)(2,1)} %param.12) | copy-start | bytes 786436
  6.5 85.9 %all-gather.6.cloned.1.call-start = ((), (), s32[]{:S(2)}) async-start(), calls=%async_computation | async-start | bytes 5242880 | tf_op jit(solution)/shard_map/all_gather | solution.py:36
  7.3 166.0 %all-gather.8.cloned.1.call-start = ((), (), s32[]{:S(2)}) async-start(), calls=%async_computation.1 | async-start | bytes 5242880 | tf_op jit(solution)/shard_map/all_gather | solution.py:37
  8.0 246.1 %all-gather.12.cloned.1.call-start = ((), (), s32[]{:S(2)}) async-start(), calls=%async_computation.3 | async-start | bytes 5242880 | tf_op jit(solution)/shard_map/all_gather | solution.py:38
  19.4 17.2 %collective-permute-start = (bf16[640,1024]{1,0:T(8,128)(2,1)S(1)}, bf16[640,1024]{1,0:T(8,128)(2,1)}, u32[]{:S(2)}, u32[]{:S(2)}) collective-permute-start(bf16[640,1024]{1,0:T(8,128)(2,1)S(1)} %fusion.16), channel_id=1, source_target_pairs={{0,1},{1,2},{2,3},{3,0},{4,5},{5,6},{6,7},{7,4},{8,9},{9,10},{10,1... | collective-permute-start | bytes 3932168 | tf_op jit(solution)/shard_map/ppermute | solution.py:52
  36.5 17.3 %collective-permute-start.1 = (bf16[640,1024]{1,0:T(8,128)(2,1)}, bf16[640,1024]{1,0:T(8,128)(2,1)}, u32[]{:S(2)}, u32[]{:S(2)}) collective-permute-start(bf16[640,1024]{1,0:T(8,128)(2,1)} %collective-permute-done), channel_id=1, source_target_pairs={{0,1},{1,2},{2,3},{3,0},{4,5},{5,6},{6,7},{7,4},{8,9},{9,10},{10,1... | collective-permute-start | bytes 3932168 | tf_op jit(solution)/shard_map/ppermute | solution.py:52
  36.6 235.7 %all-gather.10.cloned.1.call-start = ((), (), s32[]{:S(2)}) async-start(), calls=%async_computation.2 | async-start | bytes 1638400 | tf_op jit(solution)/shard_map/all_gather | solution.py:86
  53.9 17.3 %collective-permute-start.2 = (bf16[640,1024]{1,0:T(8,128)(2,1)}, bf16[640,1024]{1,0:T(8,128)(2,1)}, u32[]{:S(2)}, u32[]{:S(2)}) collective-permute-start(bf16[640,1024]{1,0:T(8,128)(2,1)} %collective-permute-done.1), channel_id=1, source_target_pairs={{0,1},{1,2},{2,3},{3,0},{4,5},{5,6},{6,7},{7,4},{8,9},{9,10},{10,1... | collective-permute-start | bytes 3932168 | tf_op jit(solution)/shard_map/ppermute | solution.py:52
  97.1 2.6 collective-permute-start.3
  98.4 5.6 %collective-permute-start.4 = (bf16[8,256]{1,0:T(8,128)(2,1)S(1)}, bf16[8,256]{1,0:T(8,128)(2,1)S(1)}, u32[]{:S(2)}, u32[]{:S(2)}) collective-permute-start(bf16[8,256]{1,0:T(8,128)(2,1)S(1)} %get-tuple-element.11), channel_id=1, source_target_pairs={{4,0},{8,4},{12,8},{5,1},{9,5},{13,9},{6,2},{10,6},{14,10},{7,3},{... | collective-permute-start | bytes 12296 | tf_op jit(solution)/shard_map/ppermute | solution.py:18
  178.7 201.3 %all-gather.14.cloned.1.call-start = ((), (), s32[]{:S(2)}) async-start(), calls=%async_computation.4 | async-start | bytes 1638400 | tf_op jit(solution)/shard_map/all_gather | solution.py:86
  282.3 60.1 %copy-start.3 = (bf16[2,4096,256]{2,1,0:T(8,128)(2,1)S(1)}, bf16[2,4096,256]{2,1,0:T(8,128)(2,1)}, u32[]{:S(2)}) copy-start(bf16[2,4096,256]{2,1,0:T(8,128)(2,1)} %all-gather.6.cloned.1.call-done) | copy-start | bytes 12582916
  282.3 17.1 %collective-permute-start.5 = (bf16[640,1024]{1,0:T(8,128)(2,1)S(1)}, bf16[640,1024]{1,0:T(8,128)(2,1)S(1)}, u32[]{:S(2)}, u32[]{:S(2)}) collective-permute-start(bf16[640,1024]{1,0:T(8,128)(2,1)S(1)} %fusion.20), channel_id=1, source_target_pairs={{0,1},{1,2},{2,3},{3,0},{4,5},{5,6},{6,7},{7,4},{8,9},{9,10},{10,1... | collective-permute-start | bytes 3932168 | tf_op jit(solution)/shard_map/ppermute | solution.py:52
  299.4 17.0 %collective-permute-start.6 = (bf16[640,1024]{1,0:T(8,128)(2,1)S(1)}, bf16[640,1024]{1,0:T(8,128)(2,1)S(1)}, u32[]{:S(2)}, u32[]{:S(2)}) collective-permute-start(bf16[640,1024]{1,0:T(8,128)(2,1)S(1)} %collective-permute-done.5), channel_id=1, source_target_pairs={{0,1},{1,2},{2,3},{3,0},{4,5},{5,6},{6,7},{7,4},{8,9},{9,10},{10,1... | collective-permute-start | bytes 3932168 | tf_op jit(solution)/shard_map/ppermute | solution.py:52
  316.4 17.0 %collective-permute-start.7 = (bf16[640,1024]{1,0:T(8,128)(2,1)S(1)}, bf16[640,1024]{1,0:T(8,128)(2,1)S(1)}, u32[]{:S(2)}, u32[]{:S(2)}) collective-permute-start(bf16[640,1024]{1,0:T(8,128)(2,1)S(1)} %collective-permute-done.6), channel_id=1, source_target_pairs={{0,1},{1,2},{2,3},{3,0},{4,5},{5,6},{6,7},{7,4},{8,9},{9,10},{10,1... | collective-permute-start | bytes 3932168 | tf_op jit(solution)/shard_map/ppermute | solution.py:52
  342.4 2.3 copy-start.1
  344.8 4.9 %collective-permute-start.8 = (bf16[8,256]{1,0:T(8,128)(2,1)S(1)}, bf16[8,256]{1,0:T(8,128)(2,1)S(1)}, u32[]{:S(2)}, u32[]{:S(2)}) collective-permute-start(bf16[8,256]{1,0:T(8,128)(2,1)S(1)} %get-tuple-element.8), channel_id=1, source_target_pairs={{0,4},{4,8},{8,12},{1,5},{5,9},{9,13},{2,6},{6,10},{10,14},{3,7},{... | collective-permute-start | bytes 12296 | tf_op jit(solution)/shard_map/ppermute | solution.py:17
  348.3 5.5 %collective-permute-start.9 = (bf16[8,256]{1,0:T(8,128)(2,1)S(1)}, bf16[8,256]{1,0:T(8,128)(2,1)S(1)}, u32[]{:S(2)}, u32[]{:S(2)}) collective-permute-start(bf16[8,256]{1,0:T(8,128)(2,1)S(1)} %get-tuple-element.9), channel_id=1, source_target_pairs={{4,0},{8,4},{12,8},{5,1},{9,5},{13,9},{6,2},{10,6},{14,10},{7,3},{... | collective-permute-start | bytes 12296 | tf_op jit(solution)/shard_map/ppermute | solution.py:18
Sparse Core Ops, SparseCore 0:
  8.9 83.4 all-gather.5
  94.0 79.2 all-gather.7
  174.9 79.1 all-gather.11
  255.5 16.7 all-gather.9
  361.7 18.2 all-gather.13
